TPU v7x, 512 devices: a whole 4x4x16 slice. The times are simulated.
512 devices in a mesh: sp: 64 (over z, y), tp: 8 (over x, core).
Axes of the slice: x: 4, y: 4, z: 16, core: 2. Of those that a mesh axis runs over, the one named last changes fastest.
Arguments:
- asking_matrix: bfloat16 [8192, 2048], P('sp', 'tp'), may hold values from -30 to 30
- matching_key_matrix: bfloat16 [8192, 1024], P('sp', 'tp'), may hold values from -30 to 30
- carried_value_matrix: bfloat16 [8192, 1024], P('sp', 'tp'), may hold values from -48 to 48
- silu_switch_argument: bfloat16 [8192, 2048], P('sp', 'tp'), may hold values from -6 to 6
- duality_source_matrix: bfloat16 [8192, 2048], P('sp', 'tp'), may hold values from -6 to 6
- storing_direction_matrix: bfloat16 [8192, 1024], P('sp', 'tp'), may hold values from -6 to 6
- fetching_direction_matrix: bfloat16 [8192, 1024], P('sp', 'tp'), may hold values from -6 to 6
- duality_kernel_coefficients: bfloat16 [5, 2048], P(None, 'tp'), may hold values from -2.5 to 2.5
- storing_kernel_coefficients: bfloat16 [5, 1024], P(None, 'tp'), may hold values from -2.5 to 2.5
- fetching_kernel_coefficients: bfloat16 [5, 1024], P(None, 'tp'), may hold values from -2.5 to 2.5
- raw_increment_lengths: float32 [2, 32, 8192], P(None, 'tp', 'sp'), may hold values from -5.5 to 5.5
- logarithmic_fading_speeds: float32 [2, 32], P(None, 'tp'), may hold values from -16 to -2.9
- token_fading_spikes: float32 [2, 32, 8192], P(None, 'tp', 'sp'), may hold values from -2.1 to 0
- absorber_score_vector: float32 [16], P('tp'), may hold values from 4 to 8
- cluster_scaling_factor: float32 [2048], P('tp'), may hold values from 0.1 to 1.9
- final_mapping_matrix: bfloat16 [2, 2048, 4096], P(None, 'tp', 'sp'), may hold values from -0.09375 to 0.09375
Outputs:
- mixed_out: bfloat16 [8192, 4096], P(('sp', 'tp'))
All inputs are finite; a program needn't handle non-finite values.
Results may differ from a plain program's by a relative error of at most 0.014.
Values may be sent and summed in bfloat16 or wider, within the bound.
A program may use at most 64 MiB of HBM per device.

v0:
```python
import jax
import jax.numpy as jnp
from jax import lax
from jax.sharding import Mesh
from jax.sharding import PartitionSpec as P

HEAD = 128
SSD_HEAD = 64
STATE = 128
CONV = 5
WINDOW = 128
SPAN = 128
SP = ("sp_0", "sp_1")
SP_TP = ("sp_0", "sp_1", "tp")


ROTARY_BASE = 500000.0
EPSILON = 1e-06


def padded_2(cells, sides, width):
    for axis, dim in sides:
        count = lax.axis_size(axis)
        ends = count - 1
        head = lax.slice_in_dim(cells, 0, width, axis=dim)
        tail = lax.slice_in_dim(cells, cells.shape[dim] - width, cells.shape[dim], axis=dim)
        cells = jnp.concatenate(
            [
                lax.ppermute(tail, axis, [(i, (i + 1) % count) for i in range(ends)]),
                cells,
                lax.ppermute(head, axis, [((i + 1) % count, i) for i in range(ends)]),
            ],
            axis=dim,
        )
    return cells


def nothing_yet(array, identity):
    return jax.tree.map(
        lambda a, e: jnp.broadcast_to(jnp.asarray(e, a.dtype), a.shape), array, identity
    )


def carried_in(array, axes, combine, identity, reverse):
    before = start = nothing_yet(array, identity)
    running = array
    for axis in reversed(axes):
        peers, index = (lax.axis_size(axis), lax.axis_index(axis))
        pieces = jax.tree.map(lambda part: lax.all_gather(part, axis), running)
        inside, running = (start, start)
        for k in reversed(range(peers)) if reverse else range(peers):
            passed = k > index if reverse else k < index
            running = combine(running, jax.tree.map(lambda part: part[k], pieces))
            inside = jax.tree.map(lambda new, old: jnp.where(passed, new, old), running, inside)
        before = combine(inside, before)
    return before


def gather_axes(array, axes, dim):
    result = array
    for number in range(len(axes) - 1, -1, -1):
        result = lax.all_gather(result, axes[number], axis=dim, tiled=True)
    return result


def cut_along(array, dim, peers):
    dims = array.shape
    pieces = array.reshape(*dims[:dim], peers, dims[dim] // peers, *dims[dim + 1 :])
    return jnp.moveaxis(pieces, dim, 0)


def sent_and_summed(array, axis, dim):
    pieces = cut_along(array, dim, lax.axis_size(axis))
    arrived = lax.all_to_all(pieces, axis, split_axis=0, concat_axis=0, tiled=True)
    return arrived.astype(jnp.float32).sum(axis=0)


def rotate(matrix, offset):
    row_count = matrix.shape[0]
    halfway = HEAD // 2
    heads_here = matrix.shape[1] // HEAD
    spacing = ROTARY_BASE ** (-jnp.arange(halfway, dtype=jnp.float32) * 2.0 / HEAD)
    places = (offset + jnp.arange(row_count, dtype=jnp.int32)).astype(jnp.float32)
    angles = places[:, None] * spacing[None, :]
    cosine = jnp.cos(angles)[:, None, :]
    sine_table = jnp.sin(angles)[:, None, :]
    halves = matrix.astype(jnp.float32).reshape(row_count, heads_here, 2, halfway)
    former = halves[:, :, 0]
    latter = halves[:, :, 1]
    turned = jnp.stack(
        [former * cosine - latter * sine_table, latter * cosine + former * sine_table], axis=2
    )
    return turned.reshape(row_count, heads_here * HEAD).astype(jnp.bfloat16)


def banded(matrix, block_count, kv_here):
    stacked = matrix.reshape(block_count + 2, SPAN, kv_here, HEAD)
    return jnp.concatenate([stacked[:-2], stacked[1:-1], stacked[2:]], axis=1)


def attend(turned_queries, key_band, value_band, absorber_score_vector, offset, seq_total):
    row_count = turned_queries.shape[0]
    block_count = row_count // SPAN
    kv_here = key_band.shape[1] // HEAD
    sharing = turned_queries.shape[1] // HEAD // kv_here
    key_tiles = banded(key_band, block_count, kv_here)
    value_tiles = banded(value_band, block_count, kv_here)
    query_tiles = turned_queries.reshape(block_count, SPAN, kv_here, sharing, HEAD)
    scores = jnp.einsum(
        "bqkgd,bskd->bkgqs", query_tiles, key_tiles, preferred_element_type=jnp.float32
    ) * HEAD ** (-0.5)
    within = jnp.arange(SPAN, dtype=jnp.int32)[:, None]
    across = jnp.arange(3 * SPAN, dtype=jnp.int32)[None, :]
    inside = jnp.abs(across - SPAN - within) <= WINDOW
    places = offset - SPAN + jnp.arange(block_count, dtype=jnp.int32)[:, None] * SPAN + across
    present = (places >= 0) & (places < seq_total)
    allowed = inside[None, :, :] & present[:, None, :]
    scores = jnp.where(allowed[:, None, None, :, :], scores, -jnp.inf)
    sink_rows = absorber_score_vector.reshape(kv_here, sharing)[None, :, :, None, None]
    ceiling = jnp.maximum(jnp.max(scores, axis=-1, keepdims=True), sink_rows)
    weights = jnp.exp(scores - ceiling)
    denominator = jnp.sum(weights, axis=-1, keepdims=True) + jnp.exp(sink_rows - ceiling)
    probabilities = (weights / denominator).astype(jnp.bfloat16)
    attended = jnp.einsum(
        "bkgqs,bskd->bqkgd", probabilities, value_tiles, preferred_element_type=jnp.float32
    )
    return attended.reshape(row_count, turned_queries.shape[1]).astype(jnp.bfloat16)


def convolve(padded, taps_all, row_count):
    summed = jnp.zeros((row_count, padded.shape[1]), jnp.float32)
    for tap_index in range(CONV):
        summed = summed + padded[tap_index : tap_index + row_count].astype(jnp.float32) * taps_all[
            tap_index
        ].astype(jnp.float32)
    return jax.nn.silu(summed).astype(jnp.bfloat16)


def prepare(scan_rows, step_rows, decay_rows, write_rows, read_rows):
    row_count = scan_rows.shape[0]
    block_count = row_count // SPAN
    groups_here = write_rows.shape[1]
    per_group = scan_rows.shape[2]
    highest = lax.Precision.HIGHEST
    step_tiles = step_rows.reshape(block_count, SPAN, groups_here, per_group)
    scaled = (
        scan_rows.astype(jnp.float32).reshape(block_count, SPAN, groups_here, per_group, SSD_HEAD)
        * step_tiles[..., None]
    )
    running = jnp.cumsum(decay_rows.reshape(block_count, SPAN, groups_here, per_group), axis=1)
    write_tiles = write_rows.reshape(block_count, SPAN, groups_here, STATE)
    read_tiles = read_rows.reshape(block_count, SPAN, groups_here, STATE)
    earlier_mask = jnp.arange(SPAN)[:, None] >= jnp.arange(SPAN)[None, :]
    spread = running[:, :, None] - running[:, None, :]
    fading = jnp.exp(jnp.where(earlier_mask[None, :, :, None, None], spread, -jnp.inf))
    affinity = jnp.einsum(
        "blgn,bsgn->blsg", read_tiles, write_tiles, preferred_element_type=jnp.float32
    )
    within_block = jnp.einsum(
        "blsgr,bsgrp->blgrp", affinity[..., None] * fading, scaled, precision=highest
    )
    to_end = jnp.exp(running[:, -1:] - running)
    block_states = jnp.einsum(
        "blgn,blgrp->bgrpn",
        write_tiles.astype(jnp.float32),
        scaled * to_end[..., None],
        precision=highest,
    )
    totals = running[:, -1]

    def advance(carried, block_item):
        fresh_state, block_total = block_item
        return (carried * jnp.exp(block_total)[..., None, None] + fresh_state, carried)

    final_state, entering = lax.scan(
        advance, jnp.zeros(block_states.shape[1:], jnp.float32), (block_states, totals)
    )
    summary = (jnp.exp(jnp.sum(totals, axis=0)), final_state)
    return ((within_block, entering, running, totals, read_tiles), summary)


def finish(pieces, incoming):
    within_block, entering, running, totals, read_tiles = pieces
    before = jnp.cumsum(totals, axis=0) - totals
    starting = entering + incoming[None] * jnp.exp(before)[..., None, None]
    carried = (
        jnp.einsum(
            "blgn,bgrpn->blgrp",
            read_tiles.astype(jnp.float32),
            starting,
            precision=lax.Precision.HIGHEST,
        )
        * jnp.exp(running)[..., None]
    )
    joined = within_block + carried
    return joined.reshape(joined.shape[0] * SPAN, -1)


def linked(earlier, later):
    return (earlier[0] * later[0], earlier[1] * later[0][..., None, None] + later[1])


def local(
    asking_matrix,
    matching_key_matrix,
    carried_value_matrix,
    silu_switch_argument,
    duality_source_matrix,
    storing_direction_matrix,
    fetching_direction_matrix,
    duality_kernel_coefficients,
    storing_kernel_coefficients,
    fetching_kernel_coefficients,
    raw_increment_lengths,
    logarithmic_fading_speeds,
    token_fading_spikes,
    absorber_score_vector,
    cluster_scaling_factor,
    final_mapping_matrix,
):
    row_count = asking_matrix.shape[0]
    offset = lax.axis_index(SP) * row_count
    seq_total = lax.axis_size(SP) * row_count
    turned_queries = rotate(asking_matrix, offset)
    key_value = jnp.concatenate([rotate(matching_key_matrix, offset), carried_value_matrix], axis=1)
    raw_rows = jnp.concatenate(
        [duality_source_matrix, storing_direction_matrix, fetching_direction_matrix], axis=1
    )
    margin = CONV // 2
    both_rims = padded_2(jnp.concatenate([key_value, raw_rows], axis=1), ((SP, 0),), WINDOW)
    pair_rims = both_rims[:, : key_value.shape[1]]
    raw_rims = both_rims[WINDOW - margin : WINDOW + row_count + margin, key_value.shape[1] :]
    filler = jnp.zeros((SPAN - WINDOW, key_value.shape[1]), jnp.bfloat16)
    pair_band = jnp.concatenate([filler, pair_rims, filler], axis=0)
    kv_width = matching_key_matrix.shape[1]
    attended = attend(
        turned_queries,
        pair_band[:, :kv_width],
        pair_band[:, kv_width:],
        absorber_score_vector,
        offset,
        seq_total,
    )
    conved = convolve(
        raw_rims,
        jnp.concatenate(
            [
                duality_kernel_coefficients,
                storing_kernel_coefficients,
                fetching_kernel_coefficients,
            ],
            axis=1,
        ),
        row_count,
    )
    scan_width = duality_source_matrix.shape[1]
    write_width = storing_direction_matrix.shape[1]
    groups_here = write_width // STATE
    per_group = scan_width // SSD_HEAD // groups_here
    scan_rows = conved[:, :scan_width].reshape(row_count, groups_here, per_group, SSD_HEAD)
    write_rows = conved[:, scan_width : scan_width + write_width].reshape(
        row_count, groups_here, STATE
    )
    read_rows = conved[:, scan_width + write_width :].reshape(row_count, groups_here, STATE)
    joint_increment_lengths = jax.nn.softplus(raw_increment_lengths)
    joint_fading_amounts = (
        -jnp.exp(logarithmic_fading_speeds)[:, :, None] * joint_increment_lengths
        + token_fading_spikes
    )
    steps_rows = jnp.transpose(joint_increment_lengths, (0, 2, 1)).reshape(
        2, row_count, groups_here, per_group
    )
    decay_rows = jnp.transpose(joint_fading_amounts, (0, 2, 1)).reshape(
        2, row_count, groups_here, per_group
    )
    ahead_pieces, ahead_summary = prepare(
        scan_rows, steps_rows[0], decay_rows[0], write_rows, read_rows
    )
    back_pieces, back_summary = prepare(
        scan_rows[::-1], steps_rows[1][::-1], decay_rows[1][::-1], write_rows[::-1], read_rows[::-1]
    )
    identity = (
        jnp.ones((groups_here, per_group), jnp.float32),
        jnp.zeros((groups_here, per_group, SSD_HEAD, STATE), jnp.float32),
    )
    ahead_in = carried_in(ahead_summary, SP, linked, identity, False)
    back_in = carried_in(back_summary, SP, linked, identity, True)
    both_ways = finish(ahead_pieces, ahead_in[1]) + finish(back_pieces, back_in[1])[::-1]
    gated_rows = both_ways * jax.nn.silu(silu_switch_argument.astype(jnp.float32))
    grouped = gated_rows.reshape(row_count, groups_here, -1)
    grouped = grouped * lax.rsqrt(jnp.mean(grouped * grouped, axis=-1, keepdims=True) + EPSILON)
    normed = (grouped.reshape(row_count, scan_width) * cluster_scaling_factor).astype(jnp.bfloat16)
    mixed_rows = jnp.concatenate([attended, normed], axis=1)
    whole_weight = gather_axes(final_mapping_matrix, SP, 2)
    stacked = whole_weight.reshape(-1, whole_weight.shape[2])
    return sent_and_summed(
        jnp.dot(mixed_rows, stacked, preferred_element_type=jnp.float32).astype(jnp.bfloat16),
        "tp",
        0,
    ).astype(jnp.bfloat16)


def solution(mesh):
    split = Mesh(mesh.devices.reshape(16, 4, mesh.shape["tp"]), ("sp_0", "sp_1", "tp"))
    return jax.shard_map(
        local,
        mesh=split,
        in_specs=(
            P(SP, "tp"),
            P(SP, "tp"),
            P(SP, "tp"),
            P(SP, "tp"),
            P(SP, "tp"),
            P(SP, "tp"),
            P(SP, "tp"),
            P(None, "tp"),
            P(None, "tp"),
            P(None, "tp"),
            P(None, "tp", SP),
            P(None, "tp"),
            P(None, "tp", SP),
            P("tp"),
            P("tp"),
            P(None, "tp", SP),
        ),
        out_specs=P(SP_TP, None),
        check_vma=False,
    )
```

profile of v0, /device:TPU:1, one launch (start us, length us, event | category | flops | bytes accessed | tf_op | source)
XLA Modules:
  0.0 318.4 jit_solution(13120188615834663522)
XLA Ops:
  6.6 0.9 copy.96
  7.8 0.8 constant_dynamic-update-slice_fusion.3
  8.6 0.8 constant_dynamic-update-slice_fusion.2
  9.4 0.8 constant_dynamic-update-slice_fusion.1
  10.2 0.8 constant_dynamic-update-slice_fusion
  11.0 4.0 %collective-permute-start = (bf16[128,768]{1,0:T(8,128)(2,1)S(1)}, bf16[128,768]{1,0:T(8,128)(2,1)S(1)}, u32[]{:S(2)}, u32[]{:S(2)}) collective-permute-start(bf16[128,768]{1,0:T(8,128)(2,1)S(1)} %constant_dynamic-update-slice_fusion), channel_id=1, source_target_pairs={{0,8},{8,16},{16,24},{24,32},{32,40},{40,48},{48,56},{56,64},{64,7... | collective-permute-start | bytes 589832 | tf_op jit(solution)/shard_map/ppermute | solution.py:29
  15.0 1.3 collective-permute-start.1
  17.0 0.8 fusion.243
  20.4 9.1 %all-gather.2 = f32[4,1,1,4]{3,2,1,0:T(1,128)S(1)} all-gather(f32[1,1,1,4]{3,2,1,0:T(1,128)S(1)} %get-tuple-element.51), channel_id=4, replica_groups=mesh['sp_0'=16,'sp_1'=4,'tp'=8] {'sp_1'}, dimensions={0}, use_global_device_ids=true | all-gather | bytes 80 | tf_op jit(solution)/shard_map/all_gather | solution.py:49
  29.6 1.1 multiply_convert_fusion
  31.2 10.7 %all-gather.3 = f32[16,64,128]{2,1,0:T(8,128)S(1)} all-gather(f32[4,64,128]{2,1,0:T(8,128)S(1)} %convolution_add_fusion), channel_id=5, replica_groups=mesh['sp_0'=16,'sp_1'=4,'tp'=8] {'sp_1'}, dimensions={0}, use_global_device_ids=true | all-gather | bytes 655360 | tf_op jit(solution)/shard_map/all_gather | solution.py:49
  43.0 5.7 %all-gather = f32[4,1,1,4]{3,2,1,0:T(1,128)S(1)} all-gather(f32[1,1,1,4]{3,2,1,0:T(1,128)S(1)} %get-tuple-element.55), channel_id=2, replica_groups=mesh['sp_0'=16,'sp_1'=4,'tp'=8] {'sp_1'}, dimensions={0}, use_global_device_ids=true | all-gather | bytes 80 | tf_op jit(solution)/shard_map/all_gather | solution.py:49
  49.6 9.9 %all-gather.1 = f32[16,64,128]{2,1,0:T(8,128)S(1)} all-gather(f32[4,64,128]{2,1,0:T(8,128)S(1)} %convolution_add_fusion.1), channel_id=3, replica_groups=mesh['sp_0'=16,'sp_1'=4,'tp'=8] {'sp_1'}, dimensions={0}, use_global_device_ids=true | all-gather | bytes 655360 | tf_op jit(solution)/shard_map/all_gather | solution.py:49
  60.4 10.0 %all_gather.52 = bf16[2,256,256]{1,0,2:T(2,128)(2,1)S(1)} all-gather(bf16[2,256,64]{1,0,2:T(2,128)(2,1)S(1)} %copy.117), channel_id=1, replica_groups=mesh['sp_0'=16,'sp_1'=4,'tp'=8] {'sp_1'}, dimensions={2}, use_global_device_ids=true | all-gather | bytes 327680 | tf_op jit(solution)/shard_map/all_gather | solution.py:62
  70.4 0.9 copy.118
  71.6 29.0 %all_gather.48 = f32[16,1,4]{2,1,0:T(1,128)S(1)} all-gather(f32[1,1,4]{2,1,0:T(1,128)S(1)} %get-tuple-element.100), channel_id=1, replica_groups=mesh['sp_0'=16,'sp_1'=4,'tp'=8] {'sp_0'}, dimensions={0}, use_global_device_ids=true | all-gather | bytes 272 | tf_op jit(solution)/shard_map/all_gather | solution.py:49
  100.6 22.2 %all_gather.43 = f32[16,1,4]{2,1,0:T(1,128)S(1)} all-gather(f32[1,1,4]{2,1,0:T(1,128)S(1)} %get-tuple-element.108), channel_id=1, replica_groups=mesh['sp_0'=16,'sp_1'=4,'tp'=8] {'sp_0'}, dimensions={0}, use_global_device_ids=true | all-gather | bytes 272 | tf_op jit(solution)/shard_map/all_gather | solution.py:49
  124.9 2.2 fusion.5
  128.0 58.0 %all-gather.8.cloned.1.call-done = f32[16,1,4,64,128]{4,3,2,1,0:T(8,128)} async-done(((f32[1,1,4,64,128]{4,3,2,1,0:T(8,128)}), f32[16,1,4,64,128]{4,3,2,1,0:T(8,128)}) %all-gather.8.cloned.1.call-update) | async-done | bytes 2097168 | tf_op jit(solution)/shard_map/all_gather | solution.py:49
  186.0 2.1 fusion.4
  189.1 90.2 %all-gather.12.cloned.1.call-done = bf16[2,256,4096]{2,1,0:T(8,128)(2,1)} async-done(((bf16[2,256,256]{2,1,0:T(8,128)(2,1)}), bf16[2,256,4096]{2,1,0:T(8,128)(2,1)}) %all-gather.12.cloned.1.call-update) | async-done | bytes 4194320 | tf_op jit(solution)/shard_map/all_gather | solution.py:62
  279.3 2.9 convolution_convert_fusion
  282.3 28.8 %all_to_all.5 = bf16[8,16,4096]{2,1,0:T(8,128)(2,1)S(1)} all-to-all(bf16[8,16,4096]{2,1,0:T(8,128)(2,1)S(1)} %bitcast.334), channel_id=1, replica_groups=mesh['sp_0'=16,'sp_1'=4,'tp'=8] {'tp'}, dimensions={0} | all-to-all | bytes 2097152 | tf_op jit(solution)/shard_map/all_to_all | solution.py:74
  311.1 0.8 reduce_sum.40
  (107 shorter events, 10.9 us)
Async XLA Ops:
  6.5 118.3 %all-gather.10.cloned.1.call-start = ((), (), s32[]{:S(2)}) async-start(), calls=%async_computation.2 | async-start | bytes 2228224 | tf_op jit(solution)/shard_map/all_gather | solution.py:49
  11.0 18.6 %collective-permute-start = (bf16[128,768]{1,0:T(8,128)(2,1)S(1)}, bf16[128,768]{1,0:T(8,128)(2,1)S(1)}, u32[]{:S(2)}, u32[]{:S(2)}) collective-permute-start(bf16[128,768]{1,0:T(8,128)(2,1)S(1)} %constant_dynamic-update-slice_fusion), channel_id=1, source_target_pairs={{0,8},{8,16},{16,24},{24,32},{32,40},{40,48},{48,56},{56,64},{64,7... | collective-permute-start | bytes 589832 | tf_op jit(solution)/shard_map/ppermute | solution.py:29
  15.0 14.6 %collective-permute-start.1 = (bf16[128,768]{1,0:T(8,128)(2,1)S(1)}, bf16[128,768]{1,0:T(8,128)(2,1)S(1)}, u32[]{:S(2)}, u32[]{:S(2)}) collective-permute-start(bf16[128,768]{1,0:T(8,128)(2,1)S(1)} %constant_dynamic-update-slice_fusion), channel_id=1, source_target_pairs={{8,0},{16,8},{24,16},{32,24},{40,32},{48,40},{56,48},{64,56},{72,6... | collective-permute-start | bytes 589832 | tf_op jit(solution)/shard_map/ppermute | solution.py:31
  42.0 18.3 %copy-start.2 = (bf16[2,256,64]{1,2,0:T(8,128)(2,1)S(1)}, bf16[2,256,64]{1,2,0:T(8,128)(2,1)}, u32[]{:S(2)}) copy-start(bf16[2,256,64]{1,2,0:T(8,128)(2,1)} %param.31) | copy-start | bytes 196612
  42.7 143.2 %all-gather.8.cloned.1.call-start = ((), (), s32[]{:S(2)}) async-start(), calls=%async_computation.1 | async-start | bytes 2228224 | tf_op jit(solution)/shard_map/all_gather | solution.py:49
  49.0 22.3 %copy-start.3 = (bf16[128,256]{1,0:T(8,128)(2,1)S(1)}, bf16[128,256]{1,0:T(8,128)(2,1)}, u32[]{:S(2)}) copy-start(bf16[128,256]{1,0:T(8,128)(2,1)} %param.16) | copy-start | bytes 196612
  59.5 64.2 %copy-start.6 = (f32[2]{0:T(128)S(1)}, f32[2]{0:T(128)}, u32[]{:S(2)}) copy-start(f32[2]{0:T(128)} %param.29) | copy-start | bytes 28
  60.2 63.6 %copy-start.5 = (bf16[128,128]{1,0:T(8,128)(2,1)S(1)}, bf16[128,128]{1,0:T(8,128)(2,1)}, u32[]{:S(2)}) copy-start(bf16[128,128]{1,0:T(8,128)(2,1)} %param.18) | copy-start | bytes 98308
  60.2 219.1 %all-gather.12.cloned.1.call-start = ((), (), s32[]{:S(2)}) async-start(), calls=%async_computation.3 | async-start | bytes 4456448 | tf_op jit(solution)/shard_map/all_gather | solution.py:62
  123.3 1.5 copy-start.1
  124.8 61.1 %copy-start = (f32[1,1,4,64,128]{4,3,2,1,0:T(8,128)S(1)}, f32[1,1,4,64,128]{4,3,2,1,0:T(8,128)}, u32[]{:S(2)}) copy-start(f32[1,1,4,64,128]{4,3,2,1,0:T(8,128)} %fusion.42) | copy-start | bytes 393220
  127.9 61.0 %copy-start.4 = (bf16[128,256]{1,0:T(8,128)(2,1)S(1)}, bf16[128,256]{1,0:T(8,128)(2,1)}, u32[]{:S(2)}) copy-start(bf16[128,256]{1,0:T(8,128)(2,1)} %param.19) | copy-start | bytes 196612
  186.0 3.1 copy-start.7
Sparse Core Ops, SparseCore 0:
  42.9 71.5 all-gather.9
  116.5 69.4 all-gather.7
  188.0 91.3 all-gather.11
where the time goes:
time: 319 us; the launch traced here: 318 us
  waiting for transfers between devices  148 us (46%)
  blocking collectives  125 us (39%)
  between operations  13.7 us (4%)
  matrix products  9.72 us (3%)
  local copies, waits for them, and re-layouts  9.32 us (3%)
  other arithmetic  6.57 us (2%)
  starting transfers between devices  5.4 us (2%)
    all_gather x1, waiting for transfers between devices, gather_axes(): result = lax.all_gather(result, axes[number], axis=dim, tiled=True)  90.2 us
    all_gather x6, blocking collectives, carried_in(): pieces = jax.tree.map(lambda part: lax.all_gather(part, axis), running)  86.6 us
    all_gather x2, waiting for transfers between devices, carried_in(): pieces = jax.tree.map(lambda part: lax.all_gather(part, axis), running)  58 us
    all_to_all x1, blocking collectives, sent_and_summed(): lax.all_to_all(pieces, axis, split_axis=0, concat_axis=0, tiled=True)  28.8 us
    all_gather x1, blocking collectives, gather_axes(): result = lax.all_gather(result, axes[number], axis=dim, tiled=True)  10 us
  transfers between devices with their start and end apart: 5, of which 2 were waited for; matrix products, arithmetic and copies ran while one was open for 5% of the time, Pallas kernels for 0%

commit v1 on v0

v1 whole, which is shorter than its diff:
```python
import functools

import jax
import jax.numpy as jnp
import numpy as np
from jax import lax
from jax.experimental import pallas as pl
from jax.experimental.pallas import tpu as pltpu
from jax.sharding import PartitionSpec as P

HEAD = 128
TOK = 128
CONV = 5
WINDOW = 128
NY = 4
GROUP = 8
F32 = jnp.float32
BF16 = jnp.bfloat16
ROTARY_BASE = 500000.0
EPSILON = 1e-06
HIGHEST = lax.Precision.HIGHEST


def rotary_tables(blocks):
    half = HEAD // 2
    spacing = ROTARY_BASE ** (-np.arange(half, dtype=np.float64) * 2.0 / HEAD)
    spacing = np.concatenate([spacing, spacing])
    starts = (np.arange(blocks + 2, dtype=np.float64) - 1.0)[:, None] * TOK * spacing[None, :]
    inner = np.arange(TOK, dtype=np.float64)[:, None] * spacing[None, :]
    starts = np.stack([np.cos(starts), np.sin(starts)], axis=1).astype(np.float32)
    inner = np.stack([np.cos(inner), np.sin(inner)]).astype(np.float32)
    return starts, inner


def nt(a, b, **kw):
    return lax.dot_general(a, b, (((1,), (1,)), ((), ())), preferred_element_type=F32, **kw)


def kernel(
    nz, nx,
    q_ref, k_ref, v_ref, z_ref, x_ref, b_ref, c_ref, tx_ref, tb_ref, tc_ref,
    raw_ref, spike_ref, speed_ref, sink_ref, gain_ref, w_ref, start_ref, inner_ref,
    o_ref,
    kbuf, vbuf, hx, hb, hc, pad, yw,
    s1, r1, s2, r2, s3, r3, pf, cf, pb, cb,
    wbuf, wcat, act, pbuf, prx, xbuf, xrx, fin, ybuf,
    halo_s, halo_r, w_s, w_r, s1s, s1r, s2s, s2r, s3s, s3r,
    a_s, a_r, d_s, d_r, x_s, x_r, y_s, y_r,
):
    ng = nz * NY // GROUP
    nsp = nz * NY
    sp = lax.axis_index("sp")
    tp = lax.axis_index("tp")
    m, g = lax.rem(sp, GROUP), lax.div(sp, GROUP)
    y, zz = lax.rem(sp, NY), lax.div(sp, NY)
    xx, core = lax.div(tp, 2), lax.rem(tp, 2)

    def at(s, t):
        return (s, t)

    prev = at(lax.rem(sp + nsp - 1, nsp), tp)
    nxt = at(lax.rem(sp + 1, nsp), tp)
    zprev = at(lax.rem(sp + nsp - NY, nsp), tp)
    znext = at(lax.rem(sp + NY, nsp), tp)
    partner = at(sp, tp + 1 - 2 * core)
    group_peer = [at(g * GROUP + lax.rem(m + d, GROUP), tp) for d in range(GROUP)]
    far_peer = [at(lax.rem(g + d, ng) * GROUP + m, tp) for d in range(ng)]
    y_peer = [at(zz * NY + lax.rem(y + d, NY), tp) for d in range(NY)]
    x_peer = [at(sp, lax.rem(xx + d, nx) * 2 + core) for d in range(nx)]

    barrier = pltpu.get_barrier_semaphore()
    greeted = [prev, nxt, zprev, znext, partner] + group_peer[1:] + far_peer[1:] + x_peer[1:]
    for device in greeted:
        pl.semaphore_signal(barrier, inc=1, device_id=device, device_id_type=pl.DeviceIdType.MESH)

    sends = []

    def send(src, dst, ssem, rsem, device):
        copy = pltpu.make_async_remote_copy(
            src_ref=src, dst_ref=dst, send_sem=ssem, recv_sem=rsem,
            device_id=device, device_id_type=pl.DeviceIdType.MESH,
        )
        copy.start()
        sends.append(copy)

    def arrived(dst, ssem, rsem, device):
        pltpu.make_async_remote_copy(
            src_ref=dst, dst_ref=dst, send_sem=ssem, recv_sem=rsem,
            device_id=device, device_id_type=pl.DeviceIdType.MESH,
        ).wait_recv()

    lane = lax.broadcasted_iota(jnp.int32, (TOK, 128), 1)
    sub = lax.broadcasted_iota(jnp.int32, (TOK, 128), 0)
    low = lane < 64
    low1 = low[:1]

    wbuf[zz, :, 0:64] = w_ref[0]
    wbuf[zz, :, 64:128] = w_ref[1]

    row8 = lax.broadcasted_iota(jnp.int32, (8, 128), 0)
    raw = jnp.concatenate([raw_ref[0], raw_ref[1]], axis=0)
    spike = jnp.concatenate([spike_ref[0], spike_ref[1]], axis=0)
    speed = jnp.zeros((8, 128), F32)
    for i in range(8):
        speed = jnp.where(row8 == i, speed_ref[i // 4, i % 4], speed)
    step = jnp.maximum(raw, 0.0) + jnp.log(1.0 + jnp.exp(-jnp.abs(raw)))
    logdecay = -jnp.exp(speed) * step + spike
    upto = (sub <= lane).astype(F32)
    onward = (sub >= lane).astype(F32)
    cum_f = jnp.dot(logdecay, upto, precision=HIGHEST, preferred_element_type=F32)
    cum_b = jnp.dot(logdecay, onward, precision=HIGHEST, preferred_element_type=F32)
    cum = jnp.where(row8 < 4, cum_f, cum_b)
    total = jnp.broadcast_to(jnp.sum(logdecay, axis=1, keepdims=True), (8, 128))
    to_end = step * jnp.exp(total - cum)
    grown = jnp.exp(cum)
    whole = jnp.exp(total)
    columns = jnp.concatenate([cum, to_end, grown, jnp.zeros((104, 128), F32)], axis=0).T

    def spread(first):
        tiles = [
            jnp.where(low, columns[:, first + 2 * i : first + 2 * i + 1], columns[:, first + 2 * i + 1 : first + 2 * i + 2])
            for i in range(2)
        ]
        return jnp.concatenate(tiles, axis=1)

    def spread_row(first):
        tiles = [
            jnp.where(low1, whole[first + 2 * i : first + 2 * i + 1], whole[first + 2 * i + 1 : first + 2 * i + 2])
            for i in range(2)
        ]
        return jnp.concatenate(tiles, axis=1)

    row16 = lax.broadcasted_iota(jnp.int32, (16, 256), 0)

    def split_rows(values):
        rows = jnp.zeros((16, 256), F32)
        at_row = 0
        for value in values:
            rest = value
            for _ in range(3):
                piece = rest.astype(BF16).astype(F32)
                rows = jnp.where(row16 == at_row, piece, rows)
                rest = rest - piece
                at_row += 1
        return rows.astype(BF16)

    decay_rows = split_rows([spread_row(0), spread_row(4)])

    inner_cos, inner_sin = inner_ref[0], inner_ref[1]

    def turn(value, block):
        cosine = start_ref[sp + block, 0:1, :]
        sine = start_ref[sp + block, 1:2, :]
        here_cos = cosine * inner_cos - sine * inner_sin
        here_sin = sine * inner_cos + cosine * inner_sin
        here_sin = jnp.where(low, -here_sin, here_sin)
        value = value.astype(F32)
        return (value * here_cos + pltpu.roll(value, 64, 1) * here_sin).astype(BF16)

    queries = jnp.concatenate([turn(q_ref[:, 0:128], 1), turn(q_ref[:, 128:256], 1)], axis=0)
    pad[8 : 8 + TOK, 0:256] = x_ref[...].astype(F32)
    pad[8 : 8 + TOK, 256:384] = b_ref[...].astype(F32)
    pad[8 : 8 + TOK, 384:512] = c_ref[...].astype(F32)
    r2[g] = jnp.zeros((32, 256), BF16)

    pl.semaphore_wait(barrier, len(greeted))

    for i, (ref, buf) in enumerate([(x_ref, hx), (b_ref, hb), (c_ref, hc)]):
        send(ref.at[TOK - 16 : TOK], buf.at[0], halo_s.at[2 * i], halo_r.at[2 * i], nxt)
        send(ref.at[0:16], buf.at[1], halo_s.at[2 * i + 1], halo_r.at[2 * i + 1], prev)
    right_steps, left_steps = nz // 2, nz - 1 - nz // 2
    send(wbuf.at[zz], wbuf.at[zz], w_s.at[0, 0], w_r.at[0, 1], znext)
    if left_steps:
        send(wbuf.at[zz], wbuf.at[zz], w_s.at[1, 0], w_r.at[1, 1], zprev)
    for i, (ref, buf) in enumerate([(k_ref, kbuf), (v_ref, vbuf)]):
        send(ref, buf.at[0], halo_s.at[6 + 2 * i], halo_r.at[6 + 2 * i], nxt)
        send(ref, buf.at[1], halo_s.at[7 + 2 * i], halo_r.at[7 + 2 * i], prev)

    def relay(s):
        if s <= right_steps:
            piece = lax.rem(zz + nz - s, nz)
            arrived(wbuf.at[piece], w_s.at[0, 0], w_r.at[0, s], zprev)
            if s < right_steps:
                send(wbuf.at[piece], wbuf.at[piece], w_s.at[0, s], w_r.at[0, s + 1], znext)
        if s <= left_steps:
            piece = lax.rem(zz + s, nz)
            arrived(wbuf.at[piece], w_s.at[1, 0], w_r.at[1, s], znext)
            if s < left_steps:
                send(wbuf.at[piece], wbuf.at[piece], w_s.at[1, s], w_r.at[1, s + 1], zprev)

    has_prev, has_next = sp > 0, sp < nsp - 1
    for i, (buf, first, last) in enumerate([(hx, 0, 256), (hb, 256, 384), (hc, 384, 512)]):
        arrived(buf.at[0], halo_s.at[2 * i], halo_r.at[2 * i], prev)
        arrived(buf.at[1], halo_s.at[2 * i + 1], halo_r.at[2 * i + 1], nxt)
        before = buf[0].astype(F32)[8:16]
        after = buf[1].astype(F32)[0:8]
        pad[0:8, first:last] = jnp.where(has_prev, before, 0.0)
        pad[8 + TOK : 16 + TOK, first:last] = jnp.where(has_next, after, 0.0)

    def convolved(first, last, taps_ref):
        taps = taps_ref[...].astype(F32)
        summed = jnp.zeros((TOK, last - first), F32)
        for k in range(CONV):
            summed = summed + pad[6 + k : 6 + k + TOK, first:last] * taps[k : k + 1]
        return (summed / (1.0 + jnp.exp(-summed))).astype(BF16)

    xs = convolved(0, 256, tx_ref)
    writes = convolved(256, 384, tb_ref)
    reads = convolved(384, 512, tc_ref)

    xs32 = xs.astype(F32)
    ends = jnp.concatenate([xs32 * spread(8), xs32 * spread(12)], axis=1).astype(BF16)
    states = lax.dot_general(
        writes, ends, (((0,), (0,)), ((), ())), preferred_element_type=F32
    ).astype(BF16)
    for j in range(GROUP):
        s1[j, 0:16] = states[16 * j : 16 * j + 16, 0:256]
        s1[j, 16:32] = states[16 * j : 16 * j + 16, 256:512]
        s1[j, 32:48] = decay_rows
    for d in range(1, GROUP):
        send(s1.at[lax.rem(m + d, GROUP)], r1.at[m], s1s.at[d], s1r.at[d], group_peer[d])
    r1[m] = s1[m]

    relay(1)

    for i, buf in enumerate([kbuf, vbuf]):
        arrived(buf.at[0], halo_s.at[6 + 2 * i], halo_r.at[6 + 2 * i], prev)
        arrived(buf.at[1], halo_s.at[7 + 2 * i], halo_r.at[7 + 2 * i], nxt)
    keys = jnp.concatenate([turn(kbuf[0], 0), turn(k_ref[...], 1), turn(kbuf[1], 2)], axis=0)
    values = jnp.concatenate([vbuf[0], v_ref[...], vbuf[1]], axis=0)
    scores = nt(queries, keys) * HEAD ** (-0.5)
    i_q = lax.broadcasted_iota(jnp.int32, (2 * TOK, 3 * TOK), 0) & (TOK - 1)
    j_k = lax.broadcasted_iota(jnp.int32, (2 * TOK, 3 * TOK), 1)
    first_key = jnp.where(has_prev, 0, TOK)
    last_key = jnp.where(has_next, 3 * TOK, 2 * TOK)
    allowed = (jnp.abs(j_k - TOK - i_q) <= WINDOW) & (j_k >= first_key) & (j_k < last_key)
    scores = jnp.where(allowed, scores, -1e30)
    head_row = lax.broadcasted_iota(jnp.int32, (2 * TOK, 1), 0)
    sink = jnp.where(head_row < TOK, sink_ref[0], sink_ref[1])
    top = jnp.maximum(jnp.max(scores, axis=1, keepdims=True), sink)
    weights = jnp.exp(scores - top)
    denominator = jnp.sum(weights, axis=1, keepdims=True) + jnp.exp(sink - top)
    probabilities = (weights / denominator).astype(BF16)
    attended = jnp.dot(probabilities, values, preferred_element_type=F32).astype(BF16)
    act[0, 0, :, 0:128] = attended[0:TOK]
    act[0, 0, :, 128:256] = attended[TOK : 2 * TOK]
    for d in (1, 3, 2):
        send(act.at[0, 0], act.at[NY - d, 0], a_s.at[0, d], a_r.at[0, NY - d], y_peer[d])

    relay(2)

    for d in range(1, GROUP):
        arrived(r1.at[lax.rem(m + GROUP - d, GROUP)], s1s.at[d], s1r.at[d], group_peer[d])
    fades = [r1[j, 32:48].astype(F32) for j in range(GROUP)]
    fade_f = [f[0:1] + f[1:2] + f[2:3] for f in fades]
    fade_b = [f[3:4] + f[4:5] + f[5:6] for f in fades]
    run, fade = jnp.zeros((16, 256), F32), jnp.ones((1, 256), F32)
    for j in range(GROUP):
        pf[j] = run
        cf[j] = jnp.broadcast_to(fade, (8, 256))
        run = run * fade_f[j] + r1[j, 0:16].astype(F32)
        fade = fade * fade_f[j]
    s2[0, 0:16] = run.astype(BF16)
    s2[0, 16:32] = split_rows([fade])
    run, fade = jnp.zeros((16, 256), F32), jnp.ones((1, 256), F32)
    for j in reversed(range(GROUP)):
        pb[j] = run
        cb[j] = jnp.broadcast_to(fade, (8, 256))
        run = run * fade_b[j] + r1[j, 16:32].astype(F32)
        fade = fade * fade_b[j]
    s2[1, 0:16] = run.astype(BF16)
    s2[1, 16:32] = split_rows([fade])
    for d in range(1, ng):
        other = lax.rem(g + d, ng)
        way = jnp.where(other > g, 0, 1)
        send(s2.at[way], r2.at[g], s2s.at[d], s2r.at[d], far_peer[d])

    relay(3)

    affinity = nt(reads, writes)
    for h in range(4):
        ahead = columns[:, h : h + 1] - cum[h : h + 1]
        back = columns[:, 4 + h : 5 + h] - cum[4 + h : 5 + h]
        fading = jnp.exp(jnp.where(lane <= sub, ahead, back))
        step_f, step_b = step[h : h + 1], step[4 + h : 5 + h]
        size = jnp.where(lane < sub, step_f, jnp.where(lane > sub, step_b, step_f + step_b))
        mix = (affinity * fading * size).astype(BF16)
        yw[:, 64 * h : 64 * h + 64] = jnp.dot(mix, xs[:, 64 * h : 64 * h + 64], preferred_element_type=F32)

    relay(4)
    relay(5)

    for d in range(1, ng):
        arrived(r2.at[lax.rem(g + ng - d, ng)], s2s.at[d], s2r.at[d], far_peer[d])
    come_f, come_b = jnp.zeros((16, 256), F32), jnp.zeros((16, 256), F32)
    for j in range(ng):
        f = r2[j, 16:32].astype(F32)
        come_f = jnp.where(j < g, come_f * (f[0:1] + f[1:2] + f[2:3]) + r2[j, 0:16].astype(F32), come_f)
    for j in reversed(range(ng)):
        f = r2[j, 16:32].astype(F32)
        come_b = jnp.where(j > g, come_b * (f[0:1] + f[1:2] + f[2:3]) + r2[j, 0:16].astype(F32), come_b)
    for j in range(GROUP):
        s3[j, 0:16] = (come_f * cf[j, 0:1] + pf[j]).astype(BF16)
        s3[j, 16:32] = (come_b * cb[j, 0:1] + pb[j]).astype(BF16)
    for d in range(1, GROUP):
        send(s3.at[lax.rem(m + d, GROUP)], r3.at[m], s3s.at[d], s3r.at[d], group_peer[d])
    r3[m] = s3[m]

    for s in range(6, max(right_steps, left_steps) + 1):
        relay(s)
    for p in range(nz // 2):
        one, two = wbuf[2 * p], wbuf[2 * p + 1]
        wcat[p // 2, 0:256, 128 * (p % 2) : 128 * (p % 2) + 128] = jnp.concatenate([one[:, 0:64], two[:, 0:64]], axis=1)
        wcat[p // 2, 256:512, 128 * (p % 2) : 128 * (p % 2) + 128] = jnp.concatenate([one[:, 64:128], two[:, 64:128]], axis=1)

    for d in range(1, GROUP):
        arrived(r3.at[lax.rem(m + GROUP - d, GROUP)], s3s.at[d], s3r.at[d], group_peer[d])
    in_f = r3[:, 0:16].reshape(128, 256)
    in_b = r3[:, 16:32].reshape(128, 256)
    both = (
        yw[...]
        + jnp.dot(reads, in_f, preferred_element_type=F32) * spread(16)
        + jnp.dot(reads, in_b, preferred_element_type=F32) * spread(20)
    )
    gate = z_ref[...].astype(F32)
    gated = both * (gate / (1.0 + jnp.exp(-gate)))
    mean = jnp.sum(gated * gated, axis=1, keepdims=True) * (1.0 / 256)
    act[0, 1] = (gated * lax.rsqrt(mean + EPSILON) * gain_ref[...]).astype(BF16)
    for d in (1, 3, 2):
        send(act.at[0, 1], act.at[NY - d, 1], a_s.at[1, d], a_r.at[1, NY - d], y_peer[d])

    n_cols = 64 * nz

    def pair_sum(e):
        arrived(prx.at[e], d_s.at[e], d_r.at[e], partner)
        for c in range(nx):
            rows = slice(16 * c, 16 * c + 16)
            xbuf[e, c] = (pbuf[e, core, rows].astype(F32) + prx[e, rows].astype(F32)).astype(BF16)
        for d in range(1, nx):
            send(xbuf.at[e, lax.rem(xx + d, nx)], xrx.at[e, d], x_s.at[e, d], x_r.at[e, d], x_peer[d])

    order = (0, 1, 3, 2)
    for i, e in enumerate(order):
        if e:
            arrived(act.at[e, 0], a_s.at[0, e], a_r.at[0, e], y_peer[e])
            arrived(act.at[e, 1], a_s.at[1, e], a_r.at[1, e], y_peer[e])
        for n in range(nz // 4):
            part = jnp.dot(act[e, 0], wcat[n, 0:256], preferred_element_type=F32)
            part = part + jnp.dot(act[e, 1], wcat[n, 256:512], preferred_element_type=F32)
            part = part.astype(BF16)
            for c in range(nx):
                for k in range(2):
                    pbuf[e, k, 16 * c : 16 * c + 16, 256 * n : 256 * n + 256] = part[
                        32 * c + 16 * k : 32 * c + 16 * k + 16
                    ]
        send(pbuf.at[e, 1 - core], prx.at[e], d_s.at[e], d_r.at[e], partner)
        if i:
            pair_sum(order[i - 1])
    pair_sum(order[-1])

    for e in order:
        done = xbuf[e, xx].astype(F32)
        for d in range(1, nx):
            arrived(xrx.at[e, d], x_s.at[e, d], x_r.at[e, d], x_peer[d])
            done = done + xrx[e, d].astype(F32)
        if e:
            fin[e] = done.astype(BF16)
            send(fin.at[e], ybuf.at[y], y_s.at[e], y_r.at[NY - e], y_peer[e])
        else:
            ybuf[y] = done.astype(BF16)
    for e in (1, 3, 2):
        arrived(ybuf.at[lax.rem(y + e, NY)], y_s.at[e], y_r.at[e], y_peer[e])
    for p in range(nz // 2):
        cells = [ybuf[j, :, 128 * p : 128 * p + 128] for j in range(NY)]
        for half in range(2):
            for pair in range(2):
                first = 256 * (2 * p + half) + 128 * pair
                o_ref[:, first : first + 128] = jnp.concatenate(
                    [cells[2 * pair + i][:, 64 * half : 64 * half + 64] for i in range(2)], axis=1
                )
    for copy in sends:
        copy.wait_send()


def solution(mesh):
    nz = mesh.shape["sp"] // NY
    nx = mesh.shape["tp"] // 2
    starts, inner = rotary_tables(mesh.shape["sp"])

    def local(
        asking, matching, carried, switch, source, storing, fetching,
        duality_taps, storing_taps, fetching_taps, raw, speeds, spikes, sinks, gains, mapping,
    ):
        cols = 64 * nz
        vmem = pl.BlockSpec(memory_space=pltpu.VMEM)
        smem = pl.BlockSpec(memory_space=pltpu.SMEM)
        dma = pltpu.SemaphoreType.DMA
        ng = nz * NY // GROUP
        rings = nz // 2 + 1
        scratch = [
            pltpu.VMEM((2, TOK, 128), BF16), pltpu.VMEM((2, TOK, 128), BF16),
            pltpu.VMEM((2, 16, 256), BF16), pltpu.VMEM((2, 16, 128), BF16), pltpu.VMEM((2, 16, 128), BF16),
            pltpu.VMEM((TOK + 16, 512), F32), pltpu.VMEM((TOK, 256), F32),
            pltpu.VMEM((GROUP, 48, 256), BF16), pltpu.VMEM((GROUP, 48, 256), BF16),
            pltpu.VMEM((2, 32, 256), BF16), pltpu.VMEM((ng, 32, 256), BF16),
            pltpu.VMEM((GROUP, 32, 256), BF16), pltpu.VMEM((GROUP, 32, 256), BF16),
            pltpu.VMEM((GROUP, 16, 256), F32), pltpu.VMEM((GROUP, 8, 256), F32),
            pltpu.VMEM((GROUP, 16, 256), F32), pltpu.VMEM((GROUP, 8, 256), F32),
            pltpu.VMEM((nz, 256, 128), BF16), pltpu.VMEM((nz // 4, 512, 256), BF16),
            pltpu.VMEM((NY, 2, TOK, 256), BF16),
            pltpu.VMEM((NY, 2, 16 * nx, cols), BF16), pltpu.VMEM((NY, 16 * nx, cols), BF16),
            pltpu.VMEM((NY, nx, 16, cols), BF16), pltpu.VMEM((NY, nx, 16, cols), BF16),
            pltpu.VMEM((NY, 16, cols), BF16), pltpu.VMEM((NY, 16, cols), BF16),
            dma((10,)), dma((10,)), dma((2, rings)), dma((2, rings)),
            dma((GROUP,)), dma((GROUP,)), dma((ng,)), dma((ng,)), dma((GROUP,)), dma((GROUP,)),
            dma((2, NY)), dma((2, NY)), dma((NY,)), dma((NY,)),
            dma((NY, nx)), dma((NY, nx)), dma((NY,)), dma((NY,)),
        ]
        return pl.pallas_call(
            functools.partial(kernel, nz, nx),
            out_shape=jax.ShapeDtypeStruct((TOK // (2 * nx), 4 * cols), BF16),
            in_specs=[vmem] * 12 + [smem, smem] + [vmem] * 4,
            out_specs=vmem,
            scratch_shapes=scratch,
            compiler_params=pltpu.CompilerParams(collective_id=0, has_side_effects=True),
        )(
            asking, matching, carried, switch, source, storing, fetching,
            duality_taps, storing_taps, fetching_taps, raw, spikes, speeds, sinks,
            gains.reshape(1, 256), mapping, jnp.asarray(starts), jnp.asarray(inner),
        )

    return jax.shard_map(
        local,
        mesh=mesh,
        in_specs=(
            P("sp", "tp"), P("sp", "tp"), P("sp", "tp"), P("sp", "tp"), P("sp", "tp"), P("sp", "tp"), P("sp", "tp"),
            P(None, "tp"), P(None, "tp"), P(None, "tp"),
            P(None, "tp", "sp"), P(None, "tp"), P(None, "tp", "sp"), P("tp"), P("tp"), P(None, "tp", "sp"),
        ),
        out_specs=P(("sp", "tp"), None),
        check_vma=False,
    )
```

time: 319 us -> 72.2 us (0.23)
  waiting for transfers between devices: 148 us -> 0 us
  blocking collectives: 125 us -> 0 us
  Pallas kernels: 0 us -> 68.8 us
  between operations: 13.7 us -> 0.01 us
  matrix products: 9.72 us -> 0 us
  other arithmetic: 6.57 us -> 0 us
  local copies, waits for them, and re-layouts: 9.32 us -> 3.17 us
  starting transfers between devices: 5.4 us -> 0 us
    all_gather x3 -> x0, waiting for transfers between devices: 148 us -> none  [the longest x1 90.2 us: gather_axes(): result = lax.all_gather(result, axes[number], axis=dim, tiled=True)]
    all_gather x7 -> x0, blocking collectives: 96.6 us -> none  [the longest x6 86.6 us: carried_in(): pieces = jax.tree.map(lambda part: lax.all_gather(part, axis), running)]
    pallas_call x0 -> x1, Pallas kernels: none -> 68.8 us  [local(): pl.pallas_call(functools.partial(kernel, nz, nx), out_shape=jax.ShapeDtyp...]
    all_to_all x1 -> x0, blocking collectives: 28.8 us -> none  [sent_and_summed(): lax.all_to_all(pieces, axis, split_axis=0, concat_axis=0, tiled=True)]
    dot_general x11 -> x0, matrix products: 9.72 us -> none  [the longest x2 4.32 us: finish(): jnp.einsum('blgn,bgrpn->blgrp', read_tiles.astype(jnp.float32), starting,...]
    ppermute x2 -> x0, starting transfers between devices: 5.31 us -> none  [the longest x1 4.02 us: padded_2(): lax.ppermute(tail, axis, [(i, (i + 1) % count) for i in range(ends)])]
  transfers between devices with their start and end apart: 5 -> 0, of which waited for: 2 -> 0; matrix products, arithmetic and copies ran while one was open for 5% -> 0% of each run, Pallas kernels for 0% -> 0%
where the time goes in v1:
time: 72.2 us; the launch traced here: 72 us
  Pallas kernels  68.8 us (95%)
  local copies, waits for them, and re-layouts  3.17 us (4%)
    pallas_call x1, Pallas kernels, local(): pl.pallas_call(functools.partial(kernel, nz, nx), out_shape=jax.ShapeDtyp...  68.8 us
    unnamed x2, local copies, waits for them, and re-layouts  3.17 us

profile of v1, /device:TPU:1, one launch (start us, length us, event | category | flops | bytes accessed | tf_op | source)
XLA Modules:
  0.0 72.0 jit_solution(16070296215463767793)
XLA Ops:
  0.0 1.6 %copy.19.w_ref = bf16[2,256,64]{2,1,0:T(8,128)(2,1)} copy(bf16[2,256,64]{1,2,0:T(8,128)(2,1)} %param.33) | data formatting | bytes 131072 | tf_op args[15]
  1.6 68.8 %shard_map.172 = bf16[16,4096]{1,0:T(8,128)(2,1)} custom-call(bf16[128,256]{1,0:T(8,128)(2,1)} %q_ref.1, bf16[128,128]{1,0:T(8,128)(2,1)} %k_ref.1, bf16[128,128]{1,0:T(8,128)(2,1)} %v_ref.1, bf16[128,256]{1,0:T(8,128)(2,1)} %z_ref.1, bf16[128,256]{1,0:T(8,128)(2,1)} %x_ref.1, bf16[128,128]{1,0:T(8,128)(2,1)} %b_ref.1, bf16[128,128]{1,0:T(8,128)(2,1)} %c_ref.1, ...), custom_call_target="tpu_custom_call" | custom-call | tf_op jit(solution)/shard_map/pallas_call | solution.py:419
  70.4 1.6 %copy.21 = bf16[16,4096]{1,0:T(8,128)(2,1)} copy(bf16[16,4096]{1,0:T(8,128)(2,1)} %shard_map.172) | data formatting | bytes 262144

commit v2 on v1

--- a/solution.py
+++ b/solution.py
@@ -43,9 +43,9 @@
     o_ref,
     kbuf, vbuf, hx, hb, hc, pad, yw,
     s1, r1, s2, r2, s3, r3, pf, cf, pb, cb,
-    wbuf, wcat, act, pbuf, prx, xbuf, xrx, fin, ybuf,
+    wbuf, act, pbuf, prx, xbuf, xrx, fin, ybuf,
     halo_s, halo_r, w_s, w_r, s1s, s1r, s2s, s2r, s3s, s3r,
-    a_s, a_r, d_s, d_r, x_s, x_r, y_s, y_r,
+    a_s, a_r, d_s, d_r, x_s, x_r, y_s, y_r, known_sem,
 ):
     ng = nz * NY // GROUP
     nsp = nz * NY
@@ -69,7 +69,8 @@
     x_peer = [at(sp, lax.rem(xx + d, nx) * 2 + core) for d in range(nx)]
 
     barrier = pltpu.get_barrier_semaphore()
-    greeted = [prev, nxt, zprev, znext, partner] + group_peer[1:] + far_peer[1:] + x_peer[1:]
+    known = [[at(lax.rem(sp + nsp + way * NY * hop, nsp), tp) for way in (1, -1)] for hop in (2, 4)]
+    greeted = [prev, nxt, zprev, znext, partner] + group_peer[1:] + x_peer[1:] + known[0]
     for device in greeted:
         pl.semaphore_signal(barrier, inc=1, device_id=device, device_id_type=pl.DeviceIdType.MESH)
 
@@ -94,8 +95,7 @@
     low = lane < 64
     low1 = low[:1]
 
-    wbuf[zz, :, 0:64] = w_ref[0]
-    wbuf[zz, :, 64:128] = w_ref[1]
+    wbuf[zz] = w_ref[...]
 
     row8 = lax.broadcasted_iota(jnp.int32, (8, 128), 0)
     raw = jnp.concatenate([raw_ref[0], raw_ref[1]], axis=0)
@@ -169,24 +169,28 @@
         send(ref.at[TOK - 16 : TOK], buf.at[0], halo_s.at[2 * i], halo_r.at[2 * i], nxt)
         send(ref.at[0:16], buf.at[1], halo_s.at[2 * i + 1], halo_r.at[2 * i + 1], prev)
     right_steps, left_steps = nz // 2, nz - 1 - nz // 2
-    send(wbuf.at[zz], wbuf.at[zz], w_s.at[0, 0], w_r.at[0, 1], znext)
-    if left_steps:
-        send(wbuf.at[zz], wbuf.at[zz], w_s.at[1, 0], w_r.at[1, 1], zprev)
+    for half in range(2):
+        send(w_ref.at[half], wbuf.at[zz, half], w_s.at[0, half, 0], w_r.at[0, half, 1], znext)
+        send(w_ref.at[half], wbuf.at[zz, half], w_s.at[1, half, 0], w_r.at[1, half, 1], zprev)
     for i, (ref, buf) in enumerate([(k_ref, kbuf), (v_ref, vbuf)]):
         send(ref, buf.at[0], halo_s.at[6 + 2 * i], halo_r.at[6 + 2 * i], nxt)
         send(ref, buf.at[1], halo_s.at[7 + 2 * i], halo_r.at[7 + 2 * i], prev)
 
+    def meet(rank):
+        for device in known[rank]:
+            pl.semaphore_signal(known_sem.at[rank], inc=1, device_id=device, device_id_type=pl.DeviceIdType.MESH)
+
+    meet(0)
+
     def relay(s):
-        if s <= right_steps:
-            piece = lax.rem(zz + nz - s, nz)
-            arrived(wbuf.at[piece], w_s.at[0, 0], w_r.at[0, s], zprev)
-            if s < right_steps:
-                send(wbuf.at[piece], wbuf.at[piece], w_s.at[0, s], w_r.at[0, s + 1], znext)
-        if s <= left_steps:
-            piece = lax.rem(zz + s, nz)
-            arrived(wbuf.at[piece], w_s.at[1, 0], w_r.at[1, s], znext)
-            if s < left_steps:
-                send(wbuf.at[piece], wbuf.at[piece], w_s.at[1, s], w_r.at[1, s + 1], zprev)
+        for half in range(2):
+            for way, steps, source, target in ((0, right_steps, zprev, znext), (1, left_steps, znext, zprev)):
+                if s <= steps:
+                    piece = lax.rem(zz + nz - s, nz) if way == 0 else lax.rem(zz + s, nz)
+                    block = wbuf.at[piece, half]
+                    arrived(block, w_s.at[way, half, 0], w_r.at[way, half, s], source)
+                    if s < steps:
+                        send(block, block, w_s.at[way, half, s], w_r.at[way, half, s + 1], target)
 
     has_prev, has_next = sp > 0, sp < nsp - 1
     for i, (buf, first, last) in enumerate([(hx, 0, 256), (hb, 256, 384), (hc, 384, 512)]):
@@ -207,6 +211,9 @@
     xs = convolved(0, 256, tx_ref)
     writes = convolved(256, 384, tb_ref)
     reads = convolved(384, 512, tc_ref)
+
+    pl.semaphore_wait(known_sem.at[0], 2)
+    meet(1)
 
     xs32 = xs.astype(F32)
     ends = jnp.concatenate([xs32 * spread(8), xs32 * spread(12)], axis=1).astype(BF16)
@@ -248,6 +255,7 @@
         send(act.at[0, 0], act.at[NY - d, 0], a_s.at[0, d], a_r.at[0, NY - d], y_peer[d])
 
     relay(2)
+    relay(3)
 
     for d in range(1, GROUP):
         arrived(r1.at[lax.rem(m + GROUP - d, GROUP)], s1s.at[d], s1r.at[d], group_peer[d])
@@ -270,12 +278,11 @@
         fade = fade * fade_b[j]
     s2[1, 0:16] = run.astype(BF16)
     s2[1, 16:32] = split_rows([fade])
+    pl.semaphore_wait(known_sem.at[1], 2)
     for d in range(1, ng):
         other = lax.rem(g + d, ng)
         way = jnp.where(other > g, 0, 1)
         send(s2.at[way], r2.at[g], s2s.at[d], s2r.at[d], far_peer[d])
-
-    relay(3)
 
     affinity = nt(reads, writes)
     for h in range(4):
@@ -289,6 +296,7 @@
 
     relay(4)
     relay(5)
+    relay(6)
 
     for d in range(1, ng):
         arrived(r2.at[lax.rem(g + ng - d, ng)], s2s.at[d], s2r.at[d], far_peer[d])
@@ -306,12 +314,8 @@
         send(s3.at[lax.rem(m + d, GROUP)], r3.at[m], s3s.at[d], s3r.at[d], group_peer[d])
     r3[m] = s3[m]
 
-    for s in range(6, max(right_steps, left_steps) + 1):
+    for s in range(7, right_steps + 1):
         relay(s)
-    for p in range(nz // 2):
-        one, two = wbuf[2 * p], wbuf[2 * p + 1]
-        wcat[p // 2, 0:256, 128 * (p % 2) : 128 * (p % 2) + 128] = jnp.concatenate([one[:, 0:64], two[:, 0:64]], axis=1)
-        wcat[p // 2, 256:512, 128 * (p % 2) : 128 * (p % 2) + 128] = jnp.concatenate([one[:, 64:128], two[:, 64:128]], axis=1)
 
     for d in range(1, GROUP):
         arrived(r3.at[lax.rem(m + GROUP - d, GROUP)], s3s.at[d], s3r.at[d], group_peer[d])
@@ -329,7 +333,6 @@
     for d in (1, 3, 2):
         send(act.at[0, 1], act.at[NY - d, 1], a_s.at[1, d], a_r.at[1, NY - d], y_peer[d])
 
-    n_cols = 64 * nz
 
     def pair_sum(e):
         arrived(prx.at[e], d_s.at[e], d_r.at[e], partner)
@@ -345,8 +348,8 @@
             arrived(act.at[e, 0], a_s.at[0, e], a_r.at[0, e], y_peer[e])
             arrived(act.at[e, 1], a_s.at[1, e], a_r.at[1, e], y_peer[e])
         for n in range(nz // 4):
-            part = jnp.dot(act[e, 0], wcat[n, 0:256], preferred_element_type=F32)
-            part = part + jnp.dot(act[e, 1], wcat[n, 256:512], preferred_element_type=F32)
+            part = nt(act[e, 0], wbuf[4 * n : 4 * n + 4, 0].reshape(256, 256))
+            part = part + nt(act[e, 1], wbuf[4 * n : 4 * n + 4, 1].reshape(256, 256))
             part = part.astype(BF16)
             for c in range(nx):
                 for k in range(2):
@@ -406,15 +409,15 @@
             pltpu.VMEM((GROUP, 32, 256), BF16), pltpu.VMEM((GROUP, 32, 256), BF16),
             pltpu.VMEM((GROUP, 16, 256), F32), pltpu.VMEM((GROUP, 8, 256), F32),
             pltpu.VMEM((GROUP, 16, 256), F32), pltpu.VMEM((GROUP, 8, 256), F32),
-            pltpu.VMEM((nz, 256, 128), BF16), pltpu.VMEM((nz // 4, 512, 256), BF16),
+            pltpu.VMEM((nz, 2, 64, 256), BF16),
             pltpu.VMEM((NY, 2, TOK, 256), BF16),
             pltpu.VMEM((NY, 2, 16 * nx, cols), BF16), pltpu.VMEM((NY, 16 * nx, cols), BF16),
             pltpu.VMEM((NY, nx, 16, cols), BF16), pltpu.VMEM((NY, nx, 16, cols), BF16),
             pltpu.VMEM((NY, 16, cols), BF16), pltpu.VMEM((NY, 16, cols), BF16),
-            dma((10,)), dma((10,)), dma((2, rings)), dma((2, rings)),
+            dma((10,)), dma((10,)), dma((2, 2, rings)), dma((2, 2, rings)),
             dma((GROUP,)), dma((GROUP,)), dma((ng,)), dma((ng,)), dma((GROUP,)), dma((GROUP,)),
             dma((2, NY)), dma((2, NY)), dma((NY,)), dma((NY,)),
-            dma((NY, nx)), dma((NY, nx)), dma((NY,)), dma((NY,)),
+            dma((NY, nx)), dma((NY, nx)), dma((NY,)), dma((NY,)), pltpu.SemaphoreType.REGULAR((2,)),
         ]
         return pl.pallas_call(
             functools.partial(kernel, nz, nx),
@@ -426,7 +429,7 @@
         )(
             asking, matching, carried, switch, source, storing, fetching,
             duality_taps, storing_taps, fetching_taps, raw, spikes, speeds, sinks,
-            gains.reshape(1, 256), mapping, jnp.asarray(starts), jnp.asarray(inner),
+            gains.reshape(1, 256), jnp.swapaxes(mapping, 1, 2), jnp.asarray(starts), jnp.asarray(inner),
         )
 
     return jax.shard_map(

time: 72.2 us -> 68.7 us (0.952); the launches traced: 72 us -> 67.6 us
  Pallas kernels: 68.8 us -> 66 us
  local copies, waits for them, and re-layouts: 3.17 us -> 1.57 us
    pallas_call x1, Pallas kernels: 68.8 us -> 66 us  [local(): pl.pallas_call(functools.partial(kernel, nz, nx), out_shape=jax.ShapeDtyp...]
    unnamed x2 -> x1, local copies, waits for them, and re-layouts: 3.17 us -> 1.57 us
where the time goes in v2:
time: 68.7 us; the launch traced here: 67.6 us
  Pallas kernels  66 us (96%)
  local copies, waits for them, and re-layouts  1.57 us (2%)
    pallas_call x1, Pallas kernels, local(): pl.pallas_call(functools.partial(kernel, nz, nx), out_shape=jax.ShapeDtyp...  66 us
    unnamed x1, local copies, waits for them, and re-layouts  1.57 us

profile of v2, /device:TPU:1, one launch (start us, length us, event | category | flops | bytes accessed | tf_op | source)
XLA Modules:
  0.0 67.6 jit_solution(5581214198685951042)
XLA Ops:
  0.0 66.0 %shard_map.172 = bf16[16,4096]{1,0:T(8,128)(2,1)} custom-call(bf16[128,256]{1,0:T(8,128)(2,1)} %q_ref.1, bf16[128,128]{1,0:T(8,128)(2,1)} %k_ref.1, bf16[128,128]{1,0:T(8,128)(2,1)} %v_ref.1, bf16[128,256]{1,0:T(8,128)(2,1)} %z_ref.1, bf16[128,256]{1,0:T(8,128)(2,1)} %x_ref.1, bf16[128,128]{1,0:T(8,128)(2,1)} %b_ref.1, bf16[128,128]{1,0:T(8,128)(2,1)} %c_ref.1, ...), custom_call_target="tpu_custom_call" | custom-call | tf_op jit(solution)/shard_map/pallas_call | solution.py:422
  66.0 1.6 %copy.20 = bf16[16,4096]{1,0:T(8,128)(2,1)} copy(bf16[16,4096]{1,0:T(8,128)(2,1)} %shard_map.172) | data formatting | bytes 262144

commit v3 on v1

--- a/solution.py
+++ b/solution.py
@@ -38,14 +38,16 @@
 
 def kernel(
     nz, nx,
+    q_hbm, k_hbm, v_hbm, z_hbm, x_hbm, b_hbm, c_hbm, tx_hbm, tb_hbm, tc_hbm,
+    raw_hbm, spike_hbm, speed_hbm, sink_hbm, gain_hbm, w_hbm, start_hbm, inner_hbm,
+    o_ref,
     q_ref, k_ref, v_ref, z_ref, x_ref, b_ref, c_ref, tx_ref, tb_ref, tc_ref,
-    raw_ref, spike_ref, speed_ref, sink_ref, gain_ref, w_ref, start_ref, inner_ref,
-    o_ref,
+    raw_ref, spike_ref, speed_ref, sink_ref, gain_ref, w_ref, start_ref, inner_ref, in_sem,
     kbuf, vbuf, hx, hb, hc, pad, yw,
     s1, r1, s2, r2, s3, r3, pf, cf, pb, cb,
-    wbuf, wcat, act, pbuf, prx, xbuf, xrx, fin, ybuf,
+    wbuf, act, pbuf, prx, xbuf, xrx, via, both_x, fin, ybuf,
     halo_s, halo_r, w_s, w_r, s1s, s1r, s2s, s2r, s3s, s3r,
-    a_s, a_r, d_s, d_r, x_s, x_r, y_s, y_r,
+    a_s, a_r, d_s, d_r, x_s, x_r, y_s, y_r, known_sem,
 ):
     ng = nz * NY // GROUP
     nsp = nz * NY
@@ -69,9 +71,20 @@
     x_peer = [at(sp, lax.rem(xx + d, nx) * 2 + core) for d in range(nx)]
 
     barrier = pltpu.get_barrier_semaphore()
-    greeted = [prev, nxt, zprev, znext, partner] + group_peer[1:] + far_peer[1:] + x_peer[1:]
+    known = [[at(lax.rem(sp + nsp + way * NY * hop, nsp), tp) for way in (1, -1)] for hop in (2, 4)]
+    greeted = [prev, nxt, zprev, znext, partner] + group_peer[1:] + x_peer[1:] + known[0]
     for device in greeted:
         pl.semaphore_signal(barrier, inc=1, device_id=device, device_id_type=pl.DeviceIdType.MESH)
+
+    pairs = [
+        (x_hbm, x_ref), (b_hbm, b_ref), (c_hbm, c_ref), (w_hbm, w_ref), (k_hbm, k_ref), (v_hbm, v_ref),
+        (raw_hbm, raw_ref), (spike_hbm, spike_ref), (speed_hbm, speed_ref), (q_hbm, q_ref), (inner_hbm, inner_ref),
+        (start_hbm.at[pl.ds(sp, 3)], start_ref), (tx_hbm, tx_ref), (tb_hbm, tb_ref), (tc_hbm, tc_ref),
+        (sink_hbm, sink_ref), (z_hbm, z_ref), (gain_hbm, gain_ref),
+    ]
+    inputs = [pltpu.make_async_copy(src, dst, in_sem.at[i]) for i, (src, dst) in enumerate(pairs)]
+    for copy in inputs:
+        copy.start()
 
     sends = []
 
@@ -94,15 +107,47 @@
     low = lane < 64
     low1 = low[:1]
 
-    wbuf[zz, :, 0:64] = w_ref[0]
-    wbuf[zz, :, 64:128] = w_ref[1]
+    for copy in inputs[:6]:
+        copy.wait()
+    pl.semaphore_wait(barrier, len(greeted))
+
+    for i, (ref, buf) in enumerate([(x_ref, hx), (b_ref, hb), (c_ref, hc)]):
+        send(ref.at[TOK - 16 : TOK], buf.at[0], halo_s.at[2 * i], halo_r.at[2 * i], nxt)
+        send(ref.at[0:16], buf.at[1], halo_s.at[2 * i + 1], halo_r.at[2 * i + 1], prev)
+    right_steps, left_steps = nz // 2, nz - 1 - nz // 2
+    for half in range(2):
+        send(w_ref.at[half], wbuf.at[zz, half], w_s.at[0, half, 0], w_r.at[0, half, 1], znext)
+        send(w_ref.at[half], wbuf.at[zz, half], w_s.at[1, half, 0], w_r.at[1, half, 1], zprev)
+    for i, (ref, buf) in enumerate([(k_ref, kbuf), (v_ref, vbuf)]):
+        send(ref, buf.at[0], halo_s.at[6 + 2 * i], halo_r.at[6 + 2 * i], nxt)
+        send(ref, buf.at[1], halo_s.at[7 + 2 * i], halo_r.at[7 + 2 * i], prev)
+
+    def meet(rank):
+        for device in known[rank]:
+            pl.semaphore_signal(known_sem.at[rank], inc=1, device_id=device, device_id_type=pl.DeviceIdType.MESH)
+
+    meet(0)
+
+    def relay(s):
+        for half in range(2):
+            for way, steps, source, target in ((0, right_steps, zprev, znext), (1, left_steps, znext, zprev)):
+                if s <= steps:
+                    piece = lax.rem(zz + nz - s, nz) if way == 0 else lax.rem(zz + s, nz)
+                    block = wbuf.at[piece, half]
+                    arrived(block, w_s.at[way, half, 0], w_r.at[way, half, s], source)
+                    if s < steps:
+                        send(block, block, w_s.at[way, half, s], w_r.at[way, half, s + 1], target)
+
+    for copy in inputs[6:]:
+        copy.wait()
+    wbuf[zz] = w_ref[...]
 
     row8 = lax.broadcasted_iota(jnp.int32, (8, 128), 0)
     raw = jnp.concatenate([raw_ref[0], raw_ref[1]], axis=0)
     spike = jnp.concatenate([spike_ref[0], spike_ref[1]], axis=0)
     speed = jnp.zeros((8, 128), F32)
     for i in range(8):
-        speed = jnp.where(row8 == i, speed_ref[i // 4, i % 4], speed)
+        speed = jnp.where(row8 == i, speed_ref[i // 4 : i // 4 + 1, i % 4 : i % 4 + 1], speed)
     step = jnp.maximum(raw, 0.0) + jnp.log(1.0 + jnp.exp(-jnp.abs(raw)))
     logdecay = -jnp.exp(speed) * step + spike
     upto = (sub <= lane).astype(F32)
@@ -130,27 +175,41 @@
         ]
         return jnp.concatenate(tiles, axis=1)
 
-    row16 = lax.broadcasted_iota(jnp.int32, (16, 256), 0)
+    row16 = lax.broadcasted_iota(jnp.int32, (16, 128), 0)
 
     def split_rows(values):
-        rows = jnp.zeros((16, 256), F32)
+        rows = jnp.zeros((16, 128), F32)
         at_row = 0
         for value in values:
-            rest = value
-            for _ in range(3):
-                piece = rest.astype(BF16).astype(F32)
-                rows = jnp.where(row16 == at_row, piece, rows)
-                rest = rest - piece
-                at_row += 1
+            for first in (0, 128):
+                rest = value[:, first : first + 128]
+                for _ in range(3):
+                    piece = rest.astype(BF16).astype(F32)
+                    rows = jnp.where(row16 == at_row, piece, rows)
+                    rest = rest - piece
+                    at_row += 1
         return rows.astype(BF16)
 
+    def joined_rows(rows, first):
+        rows = rows.astype(F32)
+        tiles = [rows[i : i + 1] + rows[i + 1 : i + 2] + rows[i + 2 : i + 3] for i in (first, first + 3)]
+        return jnp.concatenate(tiles, axis=1)
+
+    def wide(ref, j, first):
+        tiles = [ref[j, first + 16 * i : first + 16 * i + 16].astype(F32) for i in range(2)]
+        return jnp.concatenate(tiles, axis=1)
+
+    def narrow(ref, j, first, value):
+        for i in range(2):
+            ref[j, first + 16 * i : first + 16 * i + 16] = value[:, 128 * i : 128 * i + 128].astype(BF16)
+
     decay_rows = split_rows([spread_row(0), spread_row(4)])
 
     inner_cos, inner_sin = inner_ref[0], inner_ref[1]
 
     def turn(value, block):
-        cosine = start_ref[sp + block, 0:1, :]
-        sine = start_ref[sp + block, 1:2, :]
+        cosine = start_ref[block, 0:1, :]
+        sine = start_ref[block, 1:2, :]
         here_cos = cosine * inner_cos - sine * inner_sin
         here_sin = sine * inner_cos + cosine * inner_sin
         here_sin = jnp.where(low, -here_sin, here_sin)
@@ -161,32 +220,9 @@
     pad[8 : 8 + TOK, 0:256] = x_ref[...].astype(F32)
     pad[8 : 8 + TOK, 256:384] = b_ref[...].astype(F32)
     pad[8 : 8 + TOK, 384:512] = c_ref[...].astype(F32)
-    r2[g] = jnp.zeros((32, 256), BF16)
-
-    pl.semaphore_wait(barrier, len(greeted))
-
-    for i, (ref, buf) in enumerate([(x_ref, hx), (b_ref, hb), (c_ref, hc)]):
-        send(ref.at[TOK - 16 : TOK], buf.at[0], halo_s.at[2 * i], halo_r.at[2 * i], nxt)
-        send(ref.at[0:16], buf.at[1], halo_s.at[2 * i + 1], halo_r.at[2 * i + 1], prev)
-    right_steps, left_steps = nz // 2, nz - 1 - nz // 2
-    send(wbuf.at[zz], wbuf.at[zz], w_s.at[0, 0], w_r.at[0, 1], znext)
-    if left_steps:
-        send(wbuf.at[zz], wbuf.at[zz], w_s.at[1, 0], w_r.at[1, 1], zprev)
-    for i, (ref, buf) in enumerate([(k_ref, kbuf), (v_ref, vbuf)]):
-        send(ref, buf.at[0], halo_s.at[6 + 2 * i], halo_r.at[6 + 2 * i], nxt)
-        send(ref, buf.at[1], halo_s.at[7 + 2 * i], halo_r.at[7 + 2 * i], prev)
-
-    def relay(s):
-        if s <= right_steps:
-            piece = lax.rem(zz + nz - s, nz)
-            arrived(wbuf.at[piece], w_s.at[0, 0], w_r.at[0, s], zprev)
-            if s < right_steps:
-                send(wbuf.at[piece], wbuf.at[piece], w_s.at[0, s], w_r.at[0, s + 1], znext)
-        if s <= left_steps:
-            piece = lax.rem(zz + s, nz)
-            arrived(wbuf.at[piece], w_s.at[1, 0], w_r.at[1, s], znext)
-            if s < left_steps:
-                send(wbuf.at[piece], wbuf.at[piece], w_s.at[1, s], w_r.at[1, s + 1], zprev)
+    r2[g] = jnp.zeros((48, 128), BF16)
+
+    relay(1)
 
     has_prev, has_next = sp > 0, sp < nsp - 1
     for i, (buf, first, last) in enumerate([(hx, 0, 256), (hb, 256, 384), (hc, 384, 512)]):
@@ -214,14 +250,16 @@
         writes, ends, (((0,), (0,)), ((), ())), preferred_element_type=F32
     ).astype(BF16)
     for j in range(GROUP):
-        s1[j, 0:16] = states[16 * j : 16 * j + 16, 0:256]
-        s1[j, 16:32] = states[16 * j : 16 * j + 16, 256:512]
-        s1[j, 32:48] = decay_rows
+        for i in range(4):
+            s1[j, 16 * i : 16 * i + 16] = states[16 * j : 16 * j + 16, 128 * i : 128 * i + 128]
+        s1[j, 64:80] = decay_rows
     for d in range(1, GROUP):
         send(s1.at[lax.rem(m + d, GROUP)], r1.at[m], s1s.at[d], s1r.at[d], group_peer[d])
     r1[m] = s1[m]
-
-    relay(1)
+    pl.semaphore_wait(known_sem.at[0], 2)
+    meet(1)
+
+    relay(2)
 
     for i, buf in enumerate([kbuf, vbuf]):
         arrived(buf.at[0], halo_s.at[6 + 2 * i], halo_r.at[6 + 2 * i], prev)
@@ -236,7 +274,7 @@
     allowed = (jnp.abs(j_k - TOK - i_q) <= WINDOW) & (j_k >= first_key) & (j_k < last_key)
     scores = jnp.where(allowed, scores, -1e30)
     head_row = lax.broadcasted_iota(jnp.int32, (2 * TOK, 1), 0)
-    sink = jnp.where(head_row < TOK, sink_ref[0], sink_ref[1])
+    sink = jnp.where(head_row < TOK, sink_ref[0:1, 0:1], sink_ref[0:1, 1:2])
     top = jnp.maximum(jnp.max(scores, axis=1, keepdims=True), sink)
     weights = jnp.exp(scores - top)
     denominator = jnp.sum(weights, axis=1, keepdims=True) + jnp.exp(sink - top)
@@ -247,35 +285,33 @@
     for d in (1, 3, 2):
         send(act.at[0, 0], act.at[NY - d, 0], a_s.at[0, d], a_r.at[0, NY - d], y_peer[d])
 
-    relay(2)
+    relay(3)
 
     for d in range(1, GROUP):
         arrived(r1.at[lax.rem(m + GROUP - d, GROUP)], s1s.at[d], s1r.at[d], group_peer[d])
-    fades = [r1[j, 32:48].astype(F32) for j in range(GROUP)]
-    fade_f = [f[0:1] + f[1:2] + f[2:3] for f in fades]
-    fade_b = [f[3:4] + f[4:5] + f[5:6] for f in fades]
+    fade_f = [joined_rows(r1[j, 64:80], 0) for j in range(GROUP)]
+    fade_b = [joined_rows(r1[j, 64:80], 6) for j in range(GROUP)]
     run, fade = jnp.zeros((16, 256), F32), jnp.ones((1, 256), F32)
     for j in range(GROUP):
         pf[j] = run
         cf[j] = jnp.broadcast_to(fade, (8, 256))
-        run = run * fade_f[j] + r1[j, 0:16].astype(F32)
+        run = run * fade_f[j] + wide(r1, j, 0)
         fade = fade * fade_f[j]
-    s2[0, 0:16] = run.astype(BF16)
-    s2[0, 16:32] = split_rows([fade])
+    narrow(s2, 0, 0, run)
+    s2[0, 32:48] = split_rows([fade])
     run, fade = jnp.zeros((16, 256), F32), jnp.ones((1, 256), F32)
     for j in reversed(range(GROUP)):
         pb[j] = run
         cb[j] = jnp.broadcast_to(fade, (8, 256))
-        run = run * fade_b[j] + r1[j, 16:32].astype(F32)
+        run = run * fade_b[j] + wide(r1, j, 32)
         fade = fade * fade_b[j]
-    s2[1, 0:16] = run.astype(BF16)
-    s2[1, 16:32] = split_rows([fade])
+    narrow(s2, 1, 0, run)
+    s2[1, 32:48] = split_rows([fade])
+    pl.semaphore_wait(known_sem.at[1], 2)
     for d in range(1, ng):
         other = lax.rem(g + d, ng)
         way = jnp.where(other > g, 0, 1)
         send(s2.at[way], r2.at[g], s2s.at[d], s2r.at[d], far_peer[d])
-
-    relay(3)
 
     affinity = nt(reads, writes)
     for h in range(4):
@@ -289,34 +325,30 @@
 
     relay(4)
     relay(5)
+    relay(6)
 
     for d in range(1, ng):
         arrived(r2.at[lax.rem(g + ng - d, ng)], s2s.at[d], s2r.at[d], far_peer[d])
     come_f, come_b = jnp.zeros((16, 256), F32), jnp.zeros((16, 256), F32)
     for j in range(ng):
-        f = r2[j, 16:32].astype(F32)
-        come_f = jnp.where(j < g, come_f * (f[0:1] + f[1:2] + f[2:3]) + r2[j, 0:16].astype(F32), come_f)
+        come_f = jnp.where(j < g, come_f * joined_rows(r2[j, 32:48], 0) + wide(r2, j, 0), come_f)
     for j in reversed(range(ng)):
-        f = r2[j, 16:32].astype(F32)
-        come_b = jnp.where(j > g, come_b * (f[0:1] + f[1:2] + f[2:3]) + r2[j, 0:16].astype(F32), come_b)
+        come_b = jnp.where(j > g, come_b * joined_rows(r2[j, 32:48], 0) + wide(r2, j, 0), come_b)
     for j in range(GROUP):
-        s3[j, 0:16] = (come_f * cf[j, 0:1] + pf[j]).astype(BF16)
-        s3[j, 16:32] = (come_b * cb[j, 0:1] + pb[j]).astype(BF16)
+        narrow(s3, j, 0, come_f * cf[j, 0:1] + pf[j])
+        narrow(s3, j, 32, come_b * cb[j, 0:1] + pb[j])
     for d in range(1, GROUP):
         send(s3.at[lax.rem(m + d, GROUP)], r3.at[m], s3s.at[d], s3r.at[d], group_peer[d])
     r3[m] = s3[m]
 
-    for s in range(6, max(right_steps, left_steps) + 1):
+    for s in range(7, right_steps + 1):
         relay(s)
-    for p in range(nz // 2):
-        one, two = wbuf[2 * p], wbuf[2 * p + 1]
-        wcat[p // 2, 0:256, 128 * (p % 2) : 128 * (p % 2) + 128] = jnp.concatenate([one[:, 0:64], two[:, 0:64]], axis=1)
-        wcat[p // 2, 256:512, 128 * (p % 2) : 128 * (p % 2) + 128] = jnp.concatenate([one[:, 64:128], two[:, 64:128]], axis=1)
 
     for d in range(1, GROUP):
         arrived(r3.at[lax.rem(m + GROUP - d, GROUP)], s3s.at[d], s3r.at[d], group_peer[d])
-    in_f = r3[:, 0:16].reshape(128, 256)
-    in_b = r3[:, 16:32].reshape(128, 256)
+    tiles = [r3[:, 16 * i : 16 * i + 16].reshape(128, 128) for i in range(4)]
+    in_f = jnp.concatenate(tiles[:2], axis=1)
+    in_b = jnp.concatenate(tiles[2:], axis=1)
     both = (
         yw[...]
         + jnp.dot(reads, in_f, preferred_element_type=F32) * spread(16)
@@ -329,24 +361,40 @@
     for d in (1, 3, 2):
         send(act.at[0, 1], act.at[NY - d, 1], a_s.at[1, d], a_r.at[1, NY - d], y_peer[d])
 
-    n_cols = 64 * nz
+
+    order = (0, 1, 3, 2)
+    via_step = {0: 3, 1: 1, 3: 3, 2: 0}
+
+    def chunk(e, d):
+        return xbuf.at[e, lax.rem(xx + d, nx)]
 
     def pair_sum(e):
         arrived(prx.at[e], d_s.at[e], d_r.at[e], partner)
         for c in range(nx):
             rows = slice(16 * c, 16 * c + 16)
             xbuf[e, c] = (pbuf[e, core, rows].astype(F32) + prx[e, rows].astype(F32)).astype(BF16)
-        for d in range(1, nx):
-            send(xbuf.at[e, lax.rem(xx + d, nx)], xrx.at[e, d], x_s.at[e, d], x_r.at[e, d], x_peer[d])
-
-    order = (0, 1, 3, 2)
+        step_to = via_step[e]
+        if step_to:
+            send(chunk(e, 2), via.at[e], x_s.at[e, 2], x_r.at[e, 2], x_peer[step_to])
+            send(chunk(e, 4 - step_to), xrx.at[e, 4 - step_to], x_s.at[e, 4 - step_to], x_r.at[e, 4 - step_to], x_peer[4 - step_to])
+        else:
+            for d in (2, 1, 3):
+                send(chunk(e, d), xrx.at[e, d], x_s.at[e, d], x_r.at[e, d], x_peer[d])
+
+    def pass_on(e):
+        step_to = via_step[e]
+        if step_to:
+            arrived(via.at[e], x_s.at[e, 2], x_r.at[e, 2], x_peer[step_to])
+            both_x[e] = (xbuf[e, lax.rem(xx + step_to, nx)].astype(F32) + via[e].astype(F32)).astype(BF16)
+            send(both_x.at[e], xrx.at[e, step_to], x_s.at[e, step_to], x_r.at[e, step_to], x_peer[step_to])
+
     for i, e in enumerate(order):
         if e:
             arrived(act.at[e, 0], a_s.at[0, e], a_r.at[0, e], y_peer[e])
             arrived(act.at[e, 1], a_s.at[1, e], a_r.at[1, e], y_peer[e])
         for n in range(nz // 4):
-            part = jnp.dot(act[e, 0], wcat[n, 0:256], preferred_element_type=F32)
-            part = part + jnp.dot(act[e, 1], wcat[n, 256:512], preferred_element_type=F32)
+            part = nt(act[e, 0], wbuf[4 * n : 4 * n + 4, 0].reshape(256, 256))
+            part = part + nt(act[e, 1], wbuf[4 * n : 4 * n + 4, 1].reshape(256, 256))
             part = part.astype(BF16)
             for c in range(nx):
                 for k in range(2):
@@ -354,13 +402,16 @@
                         32 * c + 16 * k : 32 * c + 16 * k + 16
                     ]
         send(pbuf.at[e, 1 - core], prx.at[e], d_s.at[e], d_r.at[e], partner)
-        if i:
+        if i >= 1:
             pair_sum(order[i - 1])
-    pair_sum(order[-1])
+        if i >= 2:
+            pass_on(order[i - 2])
+    pair_sum(order[3])
+    pass_on(order[2])
 
     for e in order:
         done = xbuf[e, xx].astype(F32)
-        for d in range(1, nx):
+        for d in (1, 3) if via_step[e] else (1, 3, 2):
             arrived(xrx.at[e, d], x_s.at[e, d], x_r.at[e, d], x_peer[d])
             done = done + xrx[e, d].astype(F32)
         if e:
@@ -393,40 +444,47 @@
     ):
         cols = 64 * nz
         vmem = pl.BlockSpec(memory_space=pltpu.VMEM)
-        smem = pl.BlockSpec(memory_space=pltpu.SMEM)
+        hbm = pl.BlockSpec(memory_space=pltpu.HBM)
         dma = pltpu.SemaphoreType.DMA
         ng = nz * NY // GROUP
         rings = nz // 2 + 1
         scratch = [
+            pltpu.VMEM((TOK, 256), BF16), pltpu.VMEM((TOK, 128), BF16), pltpu.VMEM((TOK, 128), BF16),
+            pltpu.VMEM((TOK, 256), BF16), pltpu.VMEM((TOK, 256), BF16), pltpu.VMEM((TOK, 128), BF16),
+            pltpu.VMEM((TOK, 128), BF16), pltpu.VMEM((CONV, 256), BF16), pltpu.VMEM((CONV, 128), BF16),
+            pltpu.VMEM((CONV, 128), BF16), pltpu.VMEM((2, 4, 128), F32), pltpu.VMEM((2, 4, 128), F32),
+            pltpu.VMEM((2, 4), F32), pltpu.VMEM((1, 2), F32), pltpu.VMEM((1, 256), F32),
+            pltpu.VMEM((2, 64, 256), BF16), pltpu.VMEM((3, 2, 128), F32), pltpu.VMEM((2, TOK, 128), F32), dma((18,)),
             pltpu.VMEM((2, TOK, 128), BF16), pltpu.VMEM((2, TOK, 128), BF16),
             pltpu.VMEM((2, 16, 256), BF16), pltpu.VMEM((2, 16, 128), BF16), pltpu.VMEM((2, 16, 128), BF16),
             pltpu.VMEM((TOK + 16, 512), F32), pltpu.VMEM((TOK, 256), F32),
-            pltpu.VMEM((GROUP, 48, 256), BF16), pltpu.VMEM((GROUP, 48, 256), BF16),
-            pltpu.VMEM((2, 32, 256), BF16), pltpu.VMEM((ng, 32, 256), BF16),
-            pltpu.VMEM((GROUP, 32, 256), BF16), pltpu.VMEM((GROUP, 32, 256), BF16),
+            pltpu.VMEM((GROUP, 80, 128), BF16), pltpu.VMEM((GROUP, 80, 128), BF16),
+            pltpu.VMEM((2, 48, 128), BF16), pltpu.VMEM((ng, 48, 128), BF16),
+            pltpu.VMEM((GROUP, 64, 128), BF16), pltpu.VMEM((GROUP, 64, 128), BF16),
             pltpu.VMEM((GROUP, 16, 256), F32), pltpu.VMEM((GROUP, 8, 256), F32),
             pltpu.VMEM((GROUP, 16, 256), F32), pltpu.VMEM((GROUP, 8, 256), F32),
-            pltpu.VMEM((nz, 256, 128), BF16), pltpu.VMEM((nz // 4, 512, 256), BF16),
+            pltpu.VMEM((nz, 2, 64, 256), BF16),
             pltpu.VMEM((NY, 2, TOK, 256), BF16),
             pltpu.VMEM((NY, 2, 16 * nx, cols), BF16), pltpu.VMEM((NY, 16 * nx, cols), BF16),
             pltpu.VMEM((NY, nx, 16, cols), BF16), pltpu.VMEM((NY, nx, 16, cols), BF16),
             pltpu.VMEM((NY, 16, cols), BF16), pltpu.VMEM((NY, 16, cols), BF16),
-            dma((10,)), dma((10,)), dma((2, rings)), dma((2, rings)),
+            pltpu.VMEM((NY, 16, cols), BF16), pltpu.VMEM((NY, 16, cols), BF16),
+            dma((10,)), dma((10,)), dma((2, 2, rings)), dma((2, 2, rings)),
             dma((GROUP,)), dma((GROUP,)), dma((ng,)), dma((ng,)), dma((GROUP,)), dma((GROUP,)),
             dma((2, NY)), dma((2, NY)), dma((NY,)), dma((NY,)),
-            dma((NY, nx)), dma((NY, nx)), dma((NY,)), dma((NY,)),
+            dma((NY, nx)), dma((NY, nx)), dma((NY,)), dma((NY,)), pltpu.SemaphoreType.REGULAR((2,)),
         ]
         return pl.pallas_call(
             functools.partial(kernel, nz, nx),
             out_shape=jax.ShapeDtypeStruct((TOK // (2 * nx), 4 * cols), BF16),
-            in_specs=[vmem] * 12 + [smem, smem] + [vmem] * 4,
+            in_specs=[hbm] * 18,
             out_specs=vmem,
             scratch_shapes=scratch,
             compiler_params=pltpu.CompilerParams(collective_id=0, has_side_effects=True),
         )(
             asking, matching, carried, switch, source, storing, fetching,
-            duality_taps, storing_taps, fetching_taps, raw, spikes, speeds, sinks,
-            gains.reshape(1, 256), mapping, jnp.asarray(starts), jnp.asarray(inner),
+            duality_taps, storing_taps, fetching_taps, raw, spikes, speeds, sinks.reshape(1, 2),
+            gains.reshape(1, 256), jnp.swapaxes(mapping, 1, 2), jnp.asarray(starts), jnp.asarray(inner),
         )
 
     return jax.shard_map(

time: 72.2 us -> 65.1 us (0.902); the launches traced: 72 us -> 63.8 us
  Pallas kernels: 68.8 us -> 62.2 us
  local copies, waits for them, and re-layouts: 3.17 us -> 1.57 us
    pallas_call x1, Pallas kernels: 68.8 us -> 62.2 us  [local(): pl.pallas_call(functools.partial(kernel, nz, nx), out_shape=jax.ShapeDtyp...]
    unnamed x2 -> x1, local copies, waits for them, and re-layouts: 3.17 us -> 1.57 us
where the time goes in v3:
time: 65.1 us; the launch traced here: 63.8 us
  Pallas kernels  62.2 us (96%)
  local copies, waits for them, and re-layouts  1.57 us (2%)
    pallas_call x1, Pallas kernels, local(): pl.pallas_call(functools.partial(kernel, nz, nx), out_shape=jax.ShapeDtyp...  62.2 us
    unnamed x1, local copies, waits for them, and re-layouts  1.57 us

profile of v3, /device:TPU:1, one launch (start us, length us, event | category | flops | bytes accessed | tf_op | source)
XLA Modules:
  0.0 63.8 jit_solution(15729376745872549222)
XLA Ops:
  0.0 62.2 %shard_map.172 = bf16[16,4096]{1,0:T(8,128)(2,1)} custom-call(bf16[128,256]{1,0:T(8,128)(2,1)} %q_hbm.1, bf16[128,128]{1,0:T(8,128)(2,1)} %k_hbm.1, bf16[128,128]{1,0:T(8,128)(2,1)} %v_hbm.1, bf16[128,256]{1,0:T(8,128)(2,1)} %z_hbm.1, bf16[128,256]{1,0:T(8,128)(2,1)} %x_hbm.1, bf16[128,128]{1,0:T(8,128)(2,1)} %b_hbm.1, bf16[128,128]{1,0:T(8,128)(2,1)} %c_hbm.1, ...), custom_call_target="tpu_custom_call" | custom-call | tf_op jit(solution)/shard_map/pallas_call | solution.py:477
  62.2 1.6 %copy.20 = bf16[16,4096]{1,0:T(8,128)(2,1)} copy(bf16[16,4096]{1,0:T(8,128)(2,1)} %shard_map.172) | data formatting | bytes 262144
